TPU v7x, 256 devices: a whole 4x4x8 slice. The times are simulated.
256 devices in a mesh: ep: 64 (over z, x, core), tp: 4 (over y).
Axes of the slice: x: 4, y: 4, z: 8, core: 2. Of those that a mesh axis runs over, the one named last changes fastest.
Arguments:
- projected_queries: bfloat16 [16384, 2048], P('ep', 'tp'), may hold values from -245 to 245, as said below
- key_proj: bfloat16 [16384, 512], P('ep', 'tp'), may hold values from -6.2 to 6.2
- projected_values: bfloat16 [16384, 512], P('ep', 'tp'), may hold values from -24 to 24
- head_sink_logits: float32 [32], P('tp'), may hold values from 1 to 6
- out_weight: bfloat16 [2048, 4096], P('tp'), may hold values from -0.125 to 0.125
- expert_input: bfloat16 [8192, 4096], P('ep'), may hold values from -6 to 6
- norm_gain: float32 [4096], replicated, may hold values from 0.1 to 1.9
- routing: int32 [8192, 4], P('ep'), may hold values from 0 to 63, all different within a row; in each aligned block of 128 rows (0 to 127, 128 to 255, ...) at most 12 rows name the same one
- route_weight: float32 [8192, 4], P('ep'), may hold values from 0.1 to 1
- gate_weight: bfloat16 [64, 4096, 1024], P('ep', None, 'tp'), may hold values from -0.27929688 to 0.27929688
- up_weight: bfloat16 [64, 4096, 1024], P('ep', None, 'tp'), may hold values from -0.27929688 to 0.27929688
- down_weight: bfloat16 [64, 1024, 4096], P('ep', 'tp'), may hold values from -0.046875 to 0.046875
Outputs:
- mixer_output: bfloat16 [16384, 4096], P(('ep', 'tp'))
- expert_output: bfloat16 [8192, 4096], P('ep', 'tp')
Inputs may be any that keep to these rules, and one draw needn't show every extreme that they name: `projected_queries`: in the hidden draw some queries nearly equal a large multiple of a nearby key. `routing`: each row names 4 different experts; among the rows of one device (aligned blocks of 128 rows) no expert is named more than 12 times, a bound that some block reaches.
All inputs are finite; a program needn't handle non-finite values.
Results may differ from a plain program's by a relative error of at most 0.014.
Values may be sent and summed in bfloat16 or wider, within the bound.
A program may use at most 128 MiB of HBM per device.

v0:
```python
import jax
import jax.numpy as jnp
from jax import lax
from jax.sharding import PartitionSpec as P

D = 4096
HEAD_SIZE = 64
WINDOW_KEYS = 128
TOPK = 4
EPS = 1e-06
CLAMP = 7.0
SLOPE = 1.702


def passed_along(block, axis, distance):
    devices = range(lax.axis_size(axis))
    route = [(i - distance, i) for i in devices if i - distance in devices]
    return lax.ppermute(block, axis, route)


def shards(
    projected_queries,
    key_proj,
    projected_values,
    head_sink_logits,
    out_weight,
    expert_input,
    norm_gain,
    routing,
    route_weight,
    gate_weight,
    up_weight,
    down_weight,
):
    query_rows = projected_queries.shape[0]
    kv_heads = key_proj.shape[1] // HEAD_SIZE
    heads_per_group = projected_queries.shape[1] // HEAD_SIZE // kv_heads
    count_of_blocks = query_rows // WINDOW_KEYS
    prior_key, prior_value = passed_along(
        (key_proj[query_rows - WINDOW_KEYS :], projected_values[query_rows - WINDOW_KEYS :]),
        "ep",
        1,
    )
    key_all = jnp.concatenate([prior_key, key_proj], axis=0)
    value_all = jnp.concatenate([prior_value, projected_values], axis=0)
    window_keys = jnp.concatenate(
        [
            key_all[:-WINDOW_KEYS].reshape(count_of_blocks, WINDOW_KEYS, kv_heads, HEAD_SIZE),
            key_all[WINDOW_KEYS:].reshape(count_of_blocks, WINDOW_KEYS, kv_heads, HEAD_SIZE),
        ],
        axis=1,
    )
    window_values = jnp.concatenate(
        [
            value_all[:-WINDOW_KEYS].reshape(count_of_blocks, WINDOW_KEYS, kv_heads, HEAD_SIZE),
            value_all[WINDOW_KEYS:].reshape(count_of_blocks, WINDOW_KEYS, kv_heads, HEAD_SIZE),
        ],
        axis=1,
    )
    query_blocks = projected_queries.reshape(
        count_of_blocks, WINDOW_KEYS, kv_heads, heads_per_group, HEAD_SIZE
    )
    scores = jnp.einsum(
        "nqhgd,nshd->nhgqs", query_blocks, window_keys, preferred_element_type=jnp.float32
    ) * HEAD_SIZE ** (-0.5)
    offset = lax.axis_index("ep") * query_rows
    block_ids = jnp.arange(count_of_blocks)[:, None, None] * WINDOW_KEYS + offset
    query_pos = block_ids + jnp.arange(WINDOW_KEYS)[None, :, None]
    key_pos = block_ids - WINDOW_KEYS + jnp.arange(2 * WINDOW_KEYS)[None, None, :]
    permitted_mask = (key_pos <= query_pos) & (query_pos - key_pos < WINDOW_KEYS) & (key_pos >= 0)
    scores = jnp.where(permitted_mask[:, None, None, :, :], scores, -jnp.inf)
    sink_col = head_sink_logits.reshape(kv_heads, heads_per_group)[None, :, :, None, None]
    highest = jnp.maximum(jnp.max(scores, axis=-1, keepdims=True), sink_col)
    numerator = jnp.exp(scores - highest)
    denominator = jnp.sum(numerator, axis=-1, keepdims=True) + jnp.exp(sink_col - highest)
    weights = (numerator / denominator).astype(jnp.bfloat16)
    attended = jnp.einsum(
        "nhgqs,nshd->nqhgd", weights, window_values, preferred_element_type=jnp.float32
    )
    attended = attended.astype(jnp.bfloat16).reshape(
        query_rows, kv_heads * heads_per_group * HEAD_SIZE
    )
    mixer_output = lax.psum_scatter(
        jnp.dot(attended, out_weight, preferred_element_type=jnp.float32).astype(jnp.bfloat16),
        "tp",
        scatter_dimension=0,
        tiled=True,
    )
    token_rows = expert_input.shape[0]
    experts = lax.axis_size("ep")
    capacity = max(3 * token_rows * TOPK // (2 * experts), 2)
    col_share = D // lax.axis_size("tp")
    widened = expert_input.astype(jnp.float32)
    normed = (
        widened
        * lax.rsqrt(jnp.mean(widened * widened, axis=-1, keepdims=True) + EPS)
        * norm_gain[None, :]
    ).astype(jnp.bfloat16)
    flat_ids = routing.reshape(-1)
    onehot = (flat_ids[:, None] == jnp.arange(experts, dtype=jnp.int32)[None, :]).astype(jnp.int32)
    rank_in = jnp.cumsum(onehot, axis=0) - 1
    target = flat_ids * capacity + jnp.sum(rank_in * onehot, axis=1)
    tok_ids = jnp.arange(token_rows * TOPK) // TOPK
    slot_tok = jnp.full((experts * capacity,), token_rows, jnp.int32).at[target].set(tok_ids)
    gate_one = gate_weight[0]
    up_one = up_weight[0]
    own_cols = lax.dynamic_slice_in_dim(normed, lax.axis_index("tp") * col_share, col_share, 1)
    extended = jnp.concatenate([own_cols, jnp.zeros((1, col_share), jnp.bfloat16)], axis=0)
    outgoing = jnp.take(extended, slot_tok, axis=0).reshape(experts, capacity, col_share)
    arrived = lax.all_to_all(outgoing, "ep", split_axis=0, concat_axis=0, tiled=True).reshape(
        experts * capacity, col_share
    )
    portion = lax.all_gather(arrived, "tp", axis=1, tiled=True)
    gate_pre = jnp.dot(portion, gate_one, preferred_element_type=jnp.float32)
    up_pre = jnp.dot(portion, up_one, preferred_element_type=jnp.float32)
    gate_cut = jnp.minimum(gate_pre, CLAMP)
    activated = (
        (jnp.clip(up_pre, -CLAMP, CLAMP) + 1.0) * gate_cut * jax.nn.sigmoid(SLOPE * gate_cut)
    ).astype(jnp.bfloat16)
    down_cols = lax.all_to_all(down_weight[0], "tp", split_axis=1, concat_axis=0, tiled=True)
    expert_result = jnp.dot(
        lax.all_gather(activated, "tp", axis=1, tiled=True),
        down_cols,
        preferred_element_type=jnp.float32,
    ).astype(jnp.bfloat16)
    returned = lax.all_to_all(
        expert_result.reshape(experts, capacity, col_share),
        "ep",
        split_axis=0,
        concat_axis=0,
        tiled=True,
    )
    picked = jnp.take(returned.reshape(experts * capacity, col_share), target, axis=0)
    picked = picked.astype(jnp.float32).reshape(token_rows, TOPK, col_share)
    expert_output = jnp.sum(picked * route_weight[:, :, None], axis=1).astype(jnp.bfloat16)
    return (mixer_output, expert_output)


def solution(mesh):
    placed = (
        P("ep", "tp"),
        P("ep", "tp"),
        P("ep", "tp"),
        P("tp"),
        P("tp", None),
        P("ep", None),
        P(),
        P("ep", None),
        P("ep", None),
        P("ep", None, "tp"),
        P("ep", None, "tp"),
        P("ep", "tp", None),
    )
    return jax.shard_map(
        shards,
        mesh=mesh,
        in_specs=placed,
        out_specs=(P(("ep", "tp"), None), P("ep", "tp")),
        check_vma=False,
    )
```

profile of v0, /device:TPU:2, one launch (start us, length us, event | category | flops | bytes accessed | tf_op | source)
XLA Modules:
  0.0 303.8 jit_solution(12836123487075077681)
XLA Ops:
  7.2 2.9 convert_element_type.41
  10.9 1.2 reduce-window.6
  12.7 2.4 scatter_custom_fusion
  15.2 0.7 dynamic-slice
  15.9 1.1 fusion.25
  17.1 3.6 %gather_fusion = bf16[768,1024]{1,0:T(8,128)(2,1)} fusion(bf16[129,1024]{1,0:T(8,128)(2,1)S(1)} %concatenate.19, s32[1024]{0:T(1024)S(1)} %pad_clamp_fusion.1), kind=kCustom, calls=%fused_computation | custom fusion | bytes 3148800 | tf_op jit(solution)/shard_map/jit(_take)/gather | solution.py:109
  20.6 3.6 %gather.13 = bf16[64,12,1024]{2,1,0:T(8,128)(2,1)} reshape(bf16[768,1024]{1,0:T(8,128)(2,1)} %gather_fusion) | data formatting | bytes 3145728 | tf_op jit(solution)/shard_map/jit(_take)/gather | solution.py:109
  24.4 1.9 broadcast_select_fusion
  26.2 63.2 %all_to_all.29 = bf16[64,12,1024]{2,1,0:T(8,128)(2,1)} all-to-all(bf16[64,12,1024]{2,1,0:T(8,128)(2,1)S(1)} %broadcast_select_fusion), channel_id=1, replica_groups=mesh['ep'=64,'tp'=4] {'ep'}, dimensions={0} | all-to-all | bytes 3145728 | tf_op jit(solution)/shard_map/all_to_all | solution.py:110
  89.4 3.6 %reshape.225 = bf16[768,1024]{1,0:T(8,128)(2,1)} reshape(bf16[64,12,1024]{2,1,0:T(8,128)(2,1)} %all_to_all.29) | data formatting | bytes 3145728 | tf_op jit(solution)/shard_map/reshape | solution.py:110
  93.0 4.1 %copy.72 = bf16[1,256,4096]{1,2,0:T(8,128)(2,1)} copy(bf16[1,256,4096]{2,1,0:T(8,128)(2,1)} %param.23) | data formatting | bytes 4194304 | tf_op args[11]
  97.1 4.6 %all-to-all-start.1 = ((bf16[256,4,1024]{0,2,1:T(8,128)(2,1)}), bf16[256,4,1024]{0,2,1:T(8,128)(2,1)}, u32[]{:S(2)}, u32[]{:S(2)}) async-start(bf16[256,4,1024]{0,2,1:T(8,128)(2,1)} %bitcast.66), calls=%async_computation.2 | async-start | bytes 4194304 | tf_op jit(solution)/shard_map/all_to_all | solution.py:120
  101.8 1.9 collective-permute-start.1
  103.7 3.5 %collective-permute-start = (bf16[128,128]{1,0:T(8,128)(2,1)S(1)}, bf16[128,128]{1,0:T(8,128)(2,1)S(1)}, u32[]{:S(2)}, u32[]{:S(2)}) collective-permute-start(bf16[128,128]{1,0:T(8,128)(2,1)S(1)} %slice.18), channel_id=1, source_target_pairs={{0,4},{4,8},{8,12},{12,16},{16,20},{20,24},{24,28},{28,32},{32,36}... | collective-permute-start | bytes 98312 | tf_op jit(solution)/shard_map/ppermute | solution.py:18
  107.4 70.1 %all-gather.3.cloned.1.call-done = bf16[768,4096]{1,0:T(8,128)(2,1)} async-done(((bf16[768,1024]{1,0:T(8,128)(2,1)}), bf16[768,4096]{1,0:T(8,128)(2,1)}) %all-gather.3.cloned.1.call-update) | async-done | bytes 6291472 | tf_op jit(solution)/shard_map/all_gather | solution.py:113
  177.5 4.7 %fusion.8 = f32[768,256]{1,0:T(8,128)S(1)} fusion(bf16[768,4096]{1,0:T(8,128)(2,1)} %all-gather.3.cloned.1.call-done, bf16[1,4096,256]{2,1,0:T(8,128)(2,1)S(1)} %copy-done), kind=kOutput, calls=%fused_computation.17 | convolution fusion | flops 1610809344 | bytes 9175040 | tf_op jit(solution)/shard_map/dot_general | solution.py:114
  182.7 2.6 fusion.20
  186.9 1.9 fusion.45
  189.1 2.0 fusion.4
  191.3 0.5 fusion.23
  192.1 1.5 copy-done.2
  193.6 2.7 convolution_convert_fusion
  196.3 4.0 %copy.73 = bf16[4,256,1024]{2,1,0:T(8,128)(2,1)} copy(bf16[4,256,1024]{1,2,0:T(8,128)(2,1)} %bitcast.12) | data formatting | bytes 4194304 | tf_op jit(solution)/shard_map/all_to_all | solution.py:120
  200.3 13.5 %all-gather.5.cloned.1.call-done = bf16[768,1024]{1,0:T(8,128)(2,1)} async-done(((bf16[768,256]{1,0:T(8,128)(2,1)}), bf16[768,1024]{1,0:T(8,128)(2,1)}) %all-gather.5.cloned.1.call-update) | async-done | bytes 1572880 | tf_op jit(solution)/shard_map/all_gather | solution.py:122
  213.8 5.0 %convolution_convert_fusion.1 = bf16[768,1024]{1,0:T(8,128)(2,1)} fusion(bf16[768,1024]{1,0:T(8,128)(2,1)} %all-gather.5.cloned.1.call-done, bf16[1024,1024]{1,0:T(8,128)(2,1)} %bitcast.67), kind=kOutput, calls=%fused_computation.15 | convolution fusion | flops 1611399168 | bytes 5242880 | tf_op jit(solution)/shard_map/dot_general | solution.py:121
  218.8 3.6 %reshape.226 = bf16[64,12,1024]{2,1,0:T(8,128)(2,1)} reshape(bf16[768,1024]{1,0:T(8,128)(2,1)} %convolution_convert_fusion.1) | data formatting | bytes 3145728 | tf_op jit(solution)/shard_map/reshape | solution.py:127
  222.4 10.9 %all-to-all-start.2 = ((bf16[64,12,1024]{2,1,0:T(8,128)(2,1)}), bf16[64,12,1024]{2,1,0:T(8,128)(2,1)}, u32[]{:S(2)}, u32[]{:S(2)}) async-start(bf16[64,12,1024]{2,1,0:T(8,128)(2,1)} %reshape.226), calls=%async_computation.3 | async-start | bytes 4194304 | tf_op jit(solution)/shard_map/all_to_all | solution.py:126
  233.7 50.7 %all-to-all-done.2 = bf16[64,12,1024]{2,1,0:T(8,128)(2,1)} async-done(((bf16[64,12,1024]{2,1,0:T(8,128)(2,1)}), bf16[64,12,1024]{2,1,0:T(8,128)(2,1)}, u32[]{:S(2)}, u32[]{:S(2)}) %all-to-all-start.2) | async-done | bytes 1572896 | tf_op jit(solution)/shard_map/all_to_all | solution.py:126
  284.4 3.6 %reshape.227 = bf16[768,1024]{1,0:T(8,128)(2,1)} reshape(bf16[64,12,1024]{2,1,0:T(8,128)(2,1)} %all-to-all-done.2) | data formatting | bytes 3145728 | tf_op jit(solution)/shard_map/reshape | solution.py:133
  288.0 4.3 %gather_fusion.1 = bf16[512,1024]{1,0:T(8,128)(2,1)S(1)} fusion(bf16[768,1024]{1,0:T(8,128)(2,1)} %reshape.227, s32[1024]{0:T(1024)S(1)} %pad_clamp_fusion), kind=kCustom, calls=%fused_computation.1 | custom fusion | bytes 2099200 | tf_op jit(solution)/shard_map/jit(_take)/gather | solution.py:133
  292.4 1.2 gather.15
  293.6 3.6 %multiply_reduce_fusion = bf16[128,1024]{1,0:T(8,128)(2,1)} fusion(f32[128,4]{1,0:T(8,128)S(1)} %copy.74, bf16[128,4,1024]{2,1,0:T(4,128)(2,1)} %gather.15, pred[128,4]{1,0:T(8,128)(4,1)S(1)} %copy.70), kind=kLoop, calls=%fused_computation.9 | loop fusion | flops 1966080 | bytes 1313280 | tf_op jit(solution)/shard_map/reduce_sum | solution.py:135
  (81 shorter events, 4.8 us)
Async XLA Ops:
  7.2 170.3 %copy-start = (bf16[1,4096,256]{2,1,0:T(8,128)(2,1)S(1)}, bf16[1,4096,256]{2,1,0:T(8,128)(2,1)}, u32[]{:S(2)}) copy-start(bf16[1,4096,256]{2,1,0:T(8,128)(2,1)} %param.21) | copy-start | bytes 6291460
  7.2 3.0 copy-start.1
  7.2 170.3 %all-gather.3.cloned.1.call-start = ((), (), s32[]{:S(2)}) async-start(), calls=%async_computation.5 | async-start | bytes 7864320 | tf_op jit(solution)/shard_map/all_gather | solution.py:113
  7.2 3.2 %copy-start.7 = (s32[128,4]{0,1:T(4,128)S(1)}, s32[128,4]{0,1:T(4,128)}, u32[]{:S(2)}) copy-start(s32[128,4]{0,1:T(4,128)} %param.19) | copy-start | bytes 6148
  97.1 4.6 %copy-start.4 = (bf16[256,128]{1,0:T(8,128)(2,1)S(1)}, bf16[256,128]{1,0:T(8,128)(2,1)}, u32[]{:S(2)}) copy-start(bf16[256,128]{1,0:T(8,128)(2,1)} %param.13) | copy-start | bytes 196612
  97.1 6.6 %copy-start.5 = (bf16[256,128]{1,0:T(8,128)(2,1)S(1)}, bf16[256,128]{1,0:T(8,128)(2,1)}, u32[]{:S(2)}) copy-start(bf16[256,128]{1,0:T(8,128)(2,1)} %param.14) | copy-start | bytes 196612
  97.1 99.2 %all-to-all-start.1 = ((bf16[256,4,1024]{0,2,1:T(8,128)(2,1)}), bf16[256,4,1024]{0,2,1:T(8,128)(2,1)}, u32[]{:S(2)}, u32[]{:S(2)}) async-start(bf16[256,4,1024]{0,2,1:T(8,128)(2,1)} %bitcast.66), calls=%async_computation.2 | async-start | bytes 4194304 | tf_op jit(solution)/shard_map/all_to_all | solution.py:120
  101.7 112.1 %all-gather.5.cloned.1.call-start = ((), (), s32[]{:S(2)}) async-start(), calls=%async_computation.6 | async-start | bytes 1966080 | tf_op jit(solution)/shard_map/all_gather | solution.py:122
  101.8 84.9 %collective-permute-start.1 = (bf16[128,128]{1,0:T(8,128)(2,1)S(1)}, bf16[128,128]{1,0:T(8,128)(2,1)S(1)}, u32[]{:S(2)}, u32[]{:S(2)}) collective-permute-start(bf16[128,128]{1,0:T(8,128)(2,1)S(1)} %slice.20), channel_id=1, source_target_pairs={{0,4},{4,8},{8,12},{12,16},{16,20},{20,24},{24,28},{28,32},{32,36}... | collective-permute-start | bytes 98312 | tf_op jit(solution)/shard_map/ppermute | solution.py:18
  103.7 85.1 %collective-permute-start = (bf16[128,128]{1,0:T(8,128)(2,1)S(1)}, bf16[128,128]{1,0:T(8,128)(2,1)S(1)}, u32[]{:S(2)}, u32[]{:S(2)}) collective-permute-start(bf16[128,128]{1,0:T(8,128)(2,1)S(1)} %slice.18), channel_id=1, source_target_pairs={{0,4},{4,8},{8,12},{12,16},{16,20},{20,24},{24,28},{28,32},{32,36}... | collective-permute-start | bytes 98312 | tf_op jit(solution)/shard_map/ppermute | solution.py:18
  177.5 4.7 %copy-start.9 = (bf16[768,4096]{1,0:T(8,128)(2,1)S(1)}, bf16[768,4096]{1,0:T(8,128)(2,1)}, u32[]{:S(2)}) copy-start(bf16[768,4096]{1,0:T(8,128)(2,1)} %all-gather.3.cloned.1.call-done) | copy-start | bytes 18874372
  177.5 5.2 %copy-start.10 = (bf16[1,4096,256]{2,1,0:T(8,128)(2,1)S(1)}, bf16[1,4096,256]{2,1,0:T(8,128)(2,1)}, u32[]{:S(2)}) copy-start(bf16[1,4096,256]{2,1,0:T(8,128)(2,1)} %param.22) | copy-start | bytes 6291460
  182.7 3.4 %copy-start.6 = (bf16[256,512]{1,0:T(8,128)(2,1)S(1)}, bf16[256,512]{1,0:T(8,128)(2,1)}, u32[]{:S(2)}) copy-start(bf16[256,512]{1,0:T(8,128)(2,1)} %param.12) | copy-start | bytes 786436
  182.7 3.8 %copy-start.11 = (f32[8]{0:T(128)S(1)}, f32[8]{0:T(128)}, u32[]{:S(2)}) copy-start(f32[8]{0:T(128)} %param.15) | copy-start | bytes 100
  185.3 111.9 %reduce-scatter.2.cloned.1.call-start = ((), (), s32[]{:S(2)}) async-start(), calls=%async_computation.4 | async-start | bytes 2621440 | tf_op jit(solution)/shard_map/reduce_scatter | solution.py:83
  189.1 2.2 copy-start.3
  191.3 2.3 copy-start.2
  222.4 11.2 %copy-start.8 = (f32[128,4]{0,1:T(4,128)S(1)}, f32[128,4]{0,1:T(4,128)}, u32[]{:S(2)}) copy-start(f32[128,4]{0,1:T(4,128)} %param.20) | copy-start | bytes 6148
  222.4 62.0 %all-to-all-start.2 = ((bf16[64,12,1024]{2,1,0:T(8,128)(2,1)}), bf16[64,12,1024]{2,1,0:T(8,128)(2,1)}, u32[]{:S(2)}, u32[]{:S(2)}) async-start(bf16[64,12,1024]{2,1,0:T(8,128)(2,1)} %reshape.226), calls=%async_computation.3 | async-start | bytes 4194304 | tf_op jit(solution)/shard_map/all_to_all | solution.py:126
Sparse Core Ops, SparseCore 0:
  93.2 84.2 all-gather.2
  185.5 28.2 all-gather.4
  216.9 33.2 reduce-scatter.1
where the time goes:
time: 305 us; the launch traced here: 304 us
  waiting for transfers between devices  134 us (44%)
  blocking collectives  63.2 us (21%)
  local copies, waits for them, and re-layouts  39.7 us (13%)
  starting transfers between devices  21.2 us (7%)
  matrix products  17.4 us (6%)
  between operations  14.2 us (5%)
  other arithmetic  13.9 us (5%)
    all_gather x1, waiting for transfers between devices, shards(): portion = lax.all_gather(arrived, 'tp', axis=1, tiled=True)  70.1 us
    all_to_all x1, blocking collectives, shards(): lax.all_to_all(outgoing, 'ep', split_axis=0, concat_axis=0, tiled=True)  63.2 us
    all_to_all x1, waiting for transfers between devices, shards(): lax.all_to_all(expert_result.reshape(experts, capacity, col_share), 'ep',...  50.7 us
    all_gather x1, waiting for transfers between devices, shards(): lax.all_gather(activated, 'tp', axis=1, tiled=True)  13.5 us
    all_to_all x1, starting transfers between devices, shards(): lax.all_to_all(expert_result.reshape(experts, capacity, col_share), 'ep',...  10.9 us
    gather x2, local copies, waits for them, and re-layouts, shards(): jnp.take(extended, slot_tok, axis=0).reshape(experts, capacity, col_share)  7.16 us
    unnamed x27, local copies, waits for them, and re-layouts  6.43 us
  transfers between devices with their start and end apart: 7, of which 3 were waited for; matrix products, arithmetic and copies ran while one was open for 15% of the time, Pallas kernels for 0%

commit v1 on v0

--- a/solution.py
+++ b/solution.py
@@ -10,6 +10,27 @@
 EPS = 1e-06
 CLAMP = 7.0
 SLOPE = 1.702
+
+
+def ring_gather(shard, axis, dim):
+    size, index, rows = (lax.axis_size(axis), lax.axis_index(axis), shard.shape[dim])
+    ahead = [(i, (i + 1) % size) for i in range(size)]
+    behind = [(i, (i - 1) % size) for i in range(size)]
+    result = jnp.zeros((*shard.shape[:dim], size * rows, *shard.shape[dim + 1 :]), shard.dtype)
+    result = lax.dynamic_update_slice_in_dim(result, shard, index * rows, axis=dim)
+    from_left = from_right = shard
+    half = size // 2
+    for step in range(1, half + 1):
+        from_left = lax.ppermute(from_left, axis, ahead)
+        result = lax.dynamic_update_slice_in_dim(
+            result, from_left, (index - step) % size * rows, axis=dim
+        )
+        if step < size - half:
+            from_right = lax.ppermute(from_right, axis, behind)
+            result = lax.dynamic_update_slice_in_dim(
+                result, from_right, (index + step) % size * rows, axis=dim
+            )
+    return result
 
 
 def passed_along(block, axis, distance):
@@ -110,7 +131,7 @@
     arrived = lax.all_to_all(outgoing, "ep", split_axis=0, concat_axis=0, tiled=True).reshape(
         experts * capacity, col_share
     )
-    portion = lax.all_gather(arrived, "tp", axis=1, tiled=True)
+    portion = ring_gather(arrived, "tp", 1)
     gate_pre = jnp.dot(portion, gate_one, preferred_element_type=jnp.float32)
     up_pre = jnp.dot(portion, up_one, preferred_element_type=jnp.float32)
     gate_cut = jnp.minimum(gate_pre, CLAMP)

time: 305 us -> 294 us (0.964)
  waiting for transfers between devices: 134 us -> 117 us
  local copies, waits for them, and re-layouts: 39.7 us -> 45.8 us
    all_gather x1 -> x0, waiting for transfers between devices: 70.1 us -> none  [shards(): portion = lax.all_gather(arrived, 'tp', axis=1, tiled=True)]
    ppermute x0 -> x3, waiting for transfers between devices: none -> 52 us  [the longest x2 52 us: ring_gather(): from_left = lax.ppermute(from_left, axis, ahead)]
    dynamic_update_slice x0 -> x4, local copies, waits for them, and re-layouts: none -> 5.02 us  [the longest x2 3.21 us: ring_gather(): lax.dynamic_update_slice_in_dim(result, from_left, (index - step) % size...]
    all_to_all x1, waiting for transfers between devices: 0.01 us -> 3.58 us  [shards(): lax.all_to_all(down_weight[0], 'tp', split_axis=1, concat_axis=0, tiled=T...]
    ppermute x0 -> x3, starting transfers between devices: none -> 3.54 us  [the longest x2 1.88 us: ring_gather(): from_left = lax.ppermute(from_left, axis, ahead)]
  transfers between devices with their start and end apart: 7 -> 9, of which waited for: 3 -> 5; matrix products, arithmetic and copies ran while one was open for 15% -> 17% of each run, Pallas kernels for 0% -> 0%
where the time goes in v1:
time: 294 us; the launch traced here: 293 us
  waiting for transfers between devices  117 us (40%)
  blocking collectives  63.2 us (21%)
  local copies, waits for them, and re-layouts  45.8 us (16%)
  starting transfers between devices  23.2 us (8%)
  between operations  14.6 us (5%)
  matrix products  14.5 us (5%)
  other arithmetic  13.9 us (5%)
    all_to_all x1, blocking collectives, shards(): lax.all_to_all(outgoing, 'ep', split_axis=0, concat_axis=0, tiled=True)  63.2 us
    ppermute x2, waiting for transfers between devices, ring_gather(): from_left = lax.ppermute(from_left, axis, ahead)  52 us
    all_to_all x1, waiting for transfers between devices, shards(): lax.all_to_all(expert_result.reshape(experts, capacity, col_share), 'ep',...  50.7 us
    all_gather x1, waiting for transfers between devices, shards(): lax.all_gather(activated, 'tp', axis=1, tiled=True)  11 us
    all_to_all x1, starting transfers between devices, shards(): lax.all_to_all(expert_result.reshape(experts, capacity, col_share), 'ep',...  9.31 us
    gather x2, local copies, waits for them, and re-layouts, shards(): jnp.take(extended, slot_tok, axis=0).reshape(experts, capacity, col_share)  7.16 us
    unnamed x27, local copies, waits for them, and re-layouts  6.72 us
  transfers between devices with their start and end apart: 9, of which 5 were waited for; matrix products, arithmetic and copies ran while one was open for 17% of the time, Pallas kernels for 0%

profile of v1, /device:TPU:2, one launch (start us, length us, event | category | flops | bytes accessed | tf_op | source)
XLA Modules:
  0.0 292.5 jit_solution(1548604688542839236)
XLA Ops:
  7.2 2.9 %convert_element_type.41 = f32[128,4096]{1,0:T(8,128)} convert(bf16[128,4096]{1,0:T(8,128)(2,1)} %param.17) | non-fusion elementwise | flops 524288 | bytes 3145728 | tf_op jit(solution)/shard_map/convert_element_type | solution.py:114
  12.6 2.4 scatter_custom_fusion
  17.0 3.6 %gather_fusion = bf16[768,1024]{1,0:T(8,128)(2,1)} fusion(bf16[129,1024]{1,0:T(8,128)(2,1)S(1)} %concatenate.19, s32[1024]{0:T(1024)S(1)} %pad_clamp_fusion.1), kind=kCustom, calls=%fused_computation | custom fusion | bytes 3148800 | tf_op jit(solution)/shard_map/jit(_take)/gather | solution.py:130
  20.6 3.6 %gather.13 = bf16[64,12,1024]{2,1,0:T(8,128)(2,1)} reshape(bf16[768,1024]{1,0:T(8,128)(2,1)} %gather_fusion) | data formatting | bytes 3145728 | tf_op jit(solution)/shard_map/jit(_take)/gather | solution.py:130
  24.3 1.9 broadcast_select_fusion
  26.2 63.2 %all_to_all.29 = bf16[64,12,1024]{2,1,0:T(8,128)(2,1)} all-to-all(bf16[64,12,1024]{2,1,0:T(8,128)(2,1)S(1)} %broadcast_select_fusion), channel_id=1, replica_groups=mesh['ep'=64,'tp'=4] {'ep'}, dimensions={0} | all-to-all | bytes 3145728 | tf_op jit(solution)/shard_map/all_to_all | solution.py:131
  89.3 3.6 %reshape.225 = bf16[768,1024]{1,0:T(8,128)(2,1)} reshape(bf16[64,12,1024]{2,1,0:T(8,128)(2,1)} %all_to_all.29) | data formatting | bytes 3145728 | tf_op jit(solution)/shard_map/reshape | solution.py:131
  94.5 1.7 collective-permute-start.3
  96.2 33.0 %collective-permute-done.2 = bf16[768,1024]{1,0:T(8,128)(2,1)} collective-permute-done((bf16[768,1024]{1,0:T(8,128)(2,1)}, bf16[768,1024]{1,0:T(8,128)(2,1)}, u32[]{:S(2)}, u32[]{:S(2)}) %collective-permute-start.2) | collective-permute-done | bytes 1572896 | tf_op jit(solution)/shard_map/ppermute | solution.py:24
  129.5 4.1 %copy.72 = bf16[1,256,4096]{1,2,0:T(8,128)(2,1)} copy(bf16[1,256,4096]{2,1,0:T(8,128)(2,1)} %param.23) | data formatting | bytes 4194304 | tf_op args[11]
  133.6 4.6 %all-to-all-start.1 = ((bf16[256,4,1024]{0,2,1:T(8,128)(2,1)}), bf16[256,4,1024]{0,2,1:T(8,128)(2,1)}, u32[]{:S(2)}, u32[]{:S(2)}) async-start(bf16[256,4,1024]{0,2,1:T(8,128)(2,1)} %bitcast.66), calls=%async_computation.2 | async-start | bytes 4194304 | tf_op jit(solution)/shard_map/all_to_all | solution.py:141
  138.2 1.9 collective-permute-start.1
  140.2 3.6 %collective-permute-start = (bf16[128,128]{1,0:T(8,128)(2,1)S(1)}, bf16[128,128]{1,0:T(8,128)(2,1)S(1)}, u32[]{:S(2)}, u32[]{:S(2)}) collective-permute-start(bf16[128,128]{1,0:T(8,128)(2,1)S(1)} %slice.18), channel_id=1, source_target_pairs={{0,4},{4,8},{8,12},{12,16},{16,20},{20,24},{24,28},{28,32},{32,36}... | collective-permute-start | bytes 98312 | tf_op jit(solution)/shard_map/ppermute | solution.py:39
  145.6 1.6 constant_dynamic-update-slice_fusion.2
  147.3 1.6 constant_dynamic-update-slice_fusion.1
  148.9 19.1 %collective-permute-done.4 = bf16[768,1024]{1,0:T(8,128)(2,1)} collective-permute-done((bf16[768,1024]{1,0:T(8,128)(2,1)}, bf16[768,1024]{1,0:T(8,128)(2,1)}, u32[]{:S(2)}, u32[]{:S(2)}) %collective-permute-start.4) | collective-permute-done | bytes 1572896 | tf_op jit(solution)/shard_map/ppermute | solution.py:24
  169.6 1.8 fusion.8
  171.4 2.6 fusion.20
  175.7 1.9 fusion.45
  177.8 2.0 fusion.4
  180.8 1.6 copy-done.3
  182.5 2.7 convolution_convert_fusion
  185.2 3.6 %all-to-all-done.1 = bf16[256,4,1024]{0,2,1:T(8,128)(2,1)} async-done(((bf16[256,4,1024]{0,2,1:T(8,128)(2,1)}), bf16[256,4,1024]{0,2,1:T(8,128)(2,1)}, u32[]{:S(2)}, u32[]{:S(2)}) %all-to-all-start.1) | async-done | bytes 2097184 | tf_op jit(solution)/shard_map/all_to_all | solution.py:141
  188.7 4.0 %copy.73 = bf16[4,256,1024]{2,1,0:T(8,128)(2,1)} copy(bf16[4,256,1024]{1,2,0:T(8,128)(2,1)} %bitcast.12) | data formatting | bytes 4194304 | tf_op jit(solution)/shard_map/all_to_all | solution.py:141
  192.7 11.0 %all-gather.2.cloned.1.call-done = bf16[768,1024]{1,0:T(8,128)(2,1)} async-done(((bf16[768,256]{1,0:T(8,128)(2,1)}), bf16[768,1024]{1,0:T(8,128)(2,1)}) %all-gather.2.cloned.1.call-update) | async-done | bytes 1572880 | tf_op jit(solution)/shard_map/all_gather | solution.py:143
  203.8 5.0 %convolution_convert_fusion.1 = bf16[768,1024]{1,0:T(8,128)(2,1)} fusion(bf16[768,1024]{1,0:T(8,128)(2,1)} %all-gather.2.cloned.1.call-done, bf16[1024,1024]{1,0:T(8,128)(2,1)} %bitcast.67), kind=kOutput, calls=%fused_computation.15 | convolution fusion | flops 1611399168 | bytes 5242880 | tf_op jit(solution)/shard_map/dot_general | solution.py:142
  208.8 3.6 %reshape.226 = bf16[64,12,1024]{2,1,0:T(8,128)(2,1)} reshape(bf16[768,1024]{1,0:T(8,128)(2,1)} %convolution_convert_fusion.1) | data formatting | bytes 3145728 | tf_op jit(solution)/shard_map/reshape | solution.py:148
  212.4 9.3 %all-to-all-start.2 = ((bf16[64,12,1024]{2,1,0:T(8,128)(2,1)}), bf16[64,12,1024]{2,1,0:T(8,128)(2,1)}, u32[]{:S(2)}, u32[]{:S(2)}) async-start(bf16[64,12,1024]{2,1,0:T(8,128)(2,1)} %reshape.226), calls=%async_computation.3 | async-start | bytes 4194304 | tf_op jit(solution)/shard_map/all_to_all | solution.py:147
  222.2 50.7 %all-to-all-done.2 = bf16[64,12,1024]{2,1,0:T(8,128)(2,1)} async-done(((bf16[64,12,1024]{2,1,0:T(8,128)(2,1)}), bf16[64,12,1024]{2,1,0:T(8,128)(2,1)}, u32[]{:S(2)}, u32[]{:S(2)}) %all-to-all-start.2) | async-done | bytes 1572896 | tf_op jit(solution)/shard_map/all_to_all | solution.py:147
  272.9 3.6 %reshape.227 = bf16[768,1024]{1,0:T(8,128)(2,1)} reshape(bf16[64,12,1024]{2,1,0:T(8,128)(2,1)} %all-to-all-done.2) | data formatting | bytes 3145728 | tf_op jit(solution)/shard_map/reshape | solution.py:154
  276.5 4.3 %gather_fusion.1 = bf16[512,1024]{1,0:T(8,128)(2,1)S(1)} fusion(bf16[768,1024]{1,0:T(8,128)(2,1)} %reshape.227, s32[1024]{0:T(1024)S(1)} %pad_clamp_fusion), kind=kCustom, calls=%fused_computation.1 | custom fusion | bytes 2099200 | tf_op jit(solution)/shard_map/jit(_take)/gather | solution.py:154
  282.1 3.6 %multiply_reduce_fusion = bf16[128,1024]{1,0:T(8,128)(2,1)} fusion(f32[128,4]{1,0:T(8,128)S(1)} %copy.74, bf16[128,4,1024]{2,1,0:T(4,128)(2,1)} %gather.15, pred[128,4]{1,0:T(8,128)(4,1)S(1)} %copy.70), kind=kLoop, calls=%fused_computation.9 | loop fusion | flops 1966080 | bytes 1313280 | tf_op jit(solution)/shard_map/reduce_sum | solution.py:156
  (89 shorter events, 14.2 us)
Async XLA Ops:
  7.2 162.4 %copy-start = (bf16[1,4096,256]{2,1,0:T(8,128)(2,1)S(1)}, bf16[1,4096,256]{2,1,0:T(8,128)(2,1)}, u32[]{:S(2)}) copy-start(bf16[1,4096,256]{2,1,0:T(8,128)(2,1)} %param.21) | copy-start | bytes 6291460
  7.2 3.0 %copy-start.2 = (bf16[128,4096]{1,0:T(8,128)(2,1)S(1)}, bf16[128,4096]{1,0:T(8,128)(2,1)}, u32[]{:S(2)}) copy-start(bf16[128,4096]{1,0:T(8,128)(2,1)} %param.17) | copy-start | bytes 3145732
  7.2 3.2 %copy-start.8 = (s32[128,4]{0,1:T(4,128)S(1)}, s32[128,4]{0,1:T(4,128)}, u32[]{:S(2)}) copy-start(s32[128,4]{0,1:T(4,128)} %param.19) | copy-start | bytes 6148
  93.0 36.2 %collective-permute-start.2 = (bf16[768,1024]{1,0:T(8,128)(2,1)}, bf16[768,1024]{1,0:T(8,128)(2,1)}, u32[]{:S(2)}, u32[]{:S(2)}) collective-permute-start(bf16[768,1024]{1,0:T(8,128)(2,1)} %reshape.225), channel_id=1, source_target_pairs={{0,1},{1,2},{2,3},{3,0},{4,5},{5,6},{6,7},{7,4},{8,9},{9,10},{10,1... | collective-permute-start | bytes 4718600 | tf_op jit(solution)/shard_map/ppermute | solution.py:24
  94.5 52.7 %collective-permute-start.3 = (bf16[768,1024]{1,0:T(8,128)(2,1)}, bf16[768,1024]{1,0:T(8,128)(2,1)}, u32[]{:S(2)}, u32[]{:S(2)}) collective-permute-start(bf16[768,1024]{1,0:T(8,128)(2,1)} %reshape.225), channel_id=1, source_target_pairs={{0,3},{1,0},{2,1},{3,2},{4,7},{5,4},{6,5},{7,6},{8,11},{9,8},{10,9... | collective-permute-start | bytes 4718600 | tf_op jit(solution)/shard_map/ppermute | solution.py:29
  129.2 38.8 %collective-permute-start.4 = (bf16[768,1024]{1,0:T(8,128)(2,1)}, bf16[768,1024]{1,0:T(8,128)(2,1)}, u32[]{:S(2)}, u32[]{:S(2)}) collective-permute-start(bf16[768,1024]{1,0:T(8,128)(2,1)} %collective-permute-done.2), channel_id=1, source_target_pairs={{0,1},{1,2},{2,3},{3,0},{4,5},{5,6},{6,7},{7,4},{8,9},{9,10},{10,1... | collective-permute-start | bytes 4718600 | tf_op jit(solution)/shard_map/ppermute | solution.py:24
  133.6 4.6 %copy-start.5 = (bf16[256,128]{1,0:T(8,128)(2,1)S(1)}, bf16[256,128]{1,0:T(8,128)(2,1)}, u32[]{:S(2)}) copy-start(bf16[256,128]{1,0:T(8,128)(2,1)} %param.13) | copy-start | bytes 196612
  133.6 6.6 %copy-start.6 = (bf16[256,128]{1,0:T(8,128)(2,1)S(1)}, bf16[256,128]{1,0:T(8,128)(2,1)}, u32[]{:S(2)}) copy-start(bf16[256,128]{1,0:T(8,128)(2,1)} %param.14) | copy-start | bytes 196612
  133.6 55.2 %all-to-all-start.1 = ((bf16[256,4,1024]{0,2,1:T(8,128)(2,1)}), bf16[256,4,1024]{0,2,1:T(8,128)(2,1)}, u32[]{:S(2)}, u32[]{:S(2)}) async-start(bf16[256,4,1024]{0,2,1:T(8,128)(2,1)} %bitcast.66), calls=%async_computation.2 | async-start | bytes 4194304 | tf_op jit(solution)/shard_map/all_to_all | solution.py:141
  138.1 65.6 %all-gather.2.cloned.1.call-start = ((), (), s32[]{:S(2)}) async-start(), calls=%async_computation.5 | async-start | bytes 1966080 | tf_op jit(solution)/shard_map/all_gather | solution.py:143
  138.2 37.2 %collective-permute-start.1 = (bf16[128,128]{1,0:T(8,128)(2,1)S(1)}, bf16[128,128]{1,0:T(8,128)(2,1)S(1)}, u32[]{:S(2)}, u32[]{:S(2)}) collective-permute-start(bf16[128,128]{1,0:T(8,128)(2,1)S(1)} %slice.20), channel_id=1, source_target_pairs={{0,4},{4,8},{8,12},{12,16},{16,20},{20,24},{24,28},{28,32},{32,36}... | collective-permute-start | bytes 98312 | tf_op jit(solution)/shard_map/ppermute | solution.py:39
  140.2 37.4 %collective-permute-start = (bf16[128,128]{1,0:T(8,128)(2,1)S(1)}, bf16[128,128]{1,0:T(8,128)(2,1)S(1)}, u32[]{:S(2)}, u32[]{:S(2)}) collective-permute-start(bf16[128,128]{1,0:T(8,128)(2,1)S(1)} %slice.18), channel_id=1, source_target_pairs={{0,4},{4,8},{8,12},{12,16},{16,20},{20,24},{24,28},{28,32},{32,36}... | collective-permute-start | bytes 98312 | tf_op jit(solution)/shard_map/ppermute | solution.py:39
  144.0 1.4 copy-start.1
  169.6 1.8 copy-start.10
  171.4 3.4 %copy-start.7 = (bf16[256,512]{1,0:T(8,128)(2,1)S(1)}, bf16[256,512]{1,0:T(8,128)(2,1)}, u32[]{:S(2)}) copy-start(bf16[256,512]{1,0:T(8,128)(2,1)} %param.12) | copy-start | bytes 786436
  171.4 3.8 %copy-start.11 = (f32[8]{0:T(128)S(1)}, f32[8]{0:T(128)}, u32[]{:S(2)}) copy-start(f32[8]{0:T(128)} %param.15) | copy-start | bytes 100
  174.1 111.6 %reduce-scatter.2.cloned.1.call-start = ((), (), s32[]{:S(2)}) async-start(), calls=%async_computation.4 | async-start | bytes 2621440 | tf_op jit(solution)/shard_map/reduce_scatter | solution.py:104
  177.8 2.2 copy-start.4
  180.1 2.4 copy-start.3
  212.4 9.7 %copy-start.9 = (f32[128,4]{0,1:T(4,128)S(1)}, f32[128,4]{0,1:T(4,128)}, u32[]{:S(2)}) copy-start(f32[128,4]{0,1:T(4,128)} %param.20) | copy-start | bytes 6148
  212.4 60.5 %all-to-all-start.2 = ((bf16[64,12,1024]{2,1,0:T(8,128)(2,1)}), bf16[64,12,1024]{2,1,0:T(8,128)(2,1)}, u32[]{:S(2)}, u32[]{:S(2)}) async-start(bf16[64,12,1024]{2,1,0:T(8,128)(2,1)} %reshape.226), calls=%async_computation.3 | async-start | bytes 4194304 | tf_op jit(solution)/shard_map/all_to_all | solution.py:147
Sparse Core Ops, SparseCore 0:
  174.2 29.4 all-gather.1
  206.9 31.6 reduce-scatter.1
